TPU v7x, 32 devices: a whole 2x2x4 slice. The times are simulated.
32 devices in a mesh: tp: 8 (over z, y), dp: 4 (over x, core).
Axes of the slice: x: 2, y: 2, z: 4, core: 2. Of those that a mesh axis runs over, the one named last changes fastest.
Arguments:
- tokens: bfloat16 [192, 8448], P('dp', 'tp'), may hold values from -6 to 6
- gains: float32 [2, 8448], replicated, may hold values from 0.1 to 1.9
- w_input: bfloat16 [2, 8448, 12288], P(None, 'dp', 'tp'), may hold values from -0.0625 to 0.0625
- w_gating: bfloat16 [2, 8448, 12288], P(None, 'dp', 'tp'), may hold values from -0.0625 to 0.0625
- w_output: bfloat16 [2, 12288, 8448], P(None, 'tp'), may hold values from -0.21875 to 0.21875
- decay_rate: float32 [2, 768, 64], P(None, 'tp'), may hold values from 0.05 to 2
- frequency: float32 [2, 768, 64], P(None, 'tp'), may hold values from -3 to 3
- log_step: float32 [2, 768], P(None, 'tp'), may hold values from -2.3 to 0
- in_real: float32 [2, 768, 64, 16], P(None, 'tp'), may hold values from -1 to 1
- in_imag: float32 [2, 768, 64, 16], P(None, 'tp'), may hold values from -1 to 1
- readout_real_matrix: float32 [2, 768, 16, 64], P(None, 'tp'), may hold values from -0.5 to 0.5
- readout_imag_matrix: float32 [2, 768, 16, 64], P(None, 'tp'), may hold values from -0.5 to 0.5
- skip_gain: float32 [2, 12288], P(None, 'tp'), may hold values from -4 to 4
- state_real: float32 [2, 192, 768, 64], P(None, 'dp', 'tp'), may hold values from -6 to 6
- state_imag: float32 [2, 192, 768, 64], P(None, 'dp', 'tp'), may hold values from -6 to 6
Outputs:
- mixed: bfloat16 [192, 8448], P('dp', 'tp')
- next_real: float32 [2, 192, 768, 64], P(None, 'dp', 'tp')
- next_imag: float32 [2, 192, 768, 64], P(None, 'dp', 'tp')
All inputs are finite; a program needn't handle non-finite values.
Results may differ from a plain program's by a relative error of at most 0.008.
Values may be sent and summed in bfloat16 or wider, within the bound.
A program may use at most 256 MiB of HBM per device.

v0:
```python
import jax
import jax.numpy as jnp
from jax import lax
from jax.sharding import PartitionSpec as P

GS = 16
LAYERS = 2
PRECISION_LEVEL = lax.Precision.HIGHEST


def collect(shard):
    return lax.all_gather(shard, "tp", axis=1, tiled=True)


def spread(partial_value):
    return lax.psum_scatter(partial_value, "tp", scatter_dimension=1, tiled=True)


def on_device(
    tokens,
    gains,
    w_input,
    w_gating,
    w_output,
    decay_rate,
    frequency,
    log_step,
    in_real,
    in_imag,
    readout_real_matrix,
    readout_imag_matrix,
    skip_gain,
    state_real,
    state_imag,
):
    width = tokens.shape[1]
    offset = lax.axis_index("tp") * width
    batch = tokens.shape[0]
    groups = decay_rate.shape[1]
    shard = tokens
    whole = collect(shard)
    outs_re = []
    outs_im = []
    for layer_params in range(LAYERS):
        xf = whole.astype(jnp.float32)
        meansq = jnp.mean(xf * xf, axis=1, keepdims=True)
        inverse = lax.rsqrt(meansq + 1e-06)
        scaled = (xf * gains[layer_params][None, :]).astype(jnp.bfloat16)
        drive = jnp.dot(
            scaled,
            lax.all_gather(w_input[layer_params], "dp", axis=0, tiled=True),
            preferred_element_type=jnp.float32,
        )
        gate = jnp.dot(
            scaled,
            lax.all_gather(w_gating[layer_params], "dp", axis=0, tiled=True),
            preferred_element_type=jnp.float32,
        )
        drive = drive * inverse
        gate = gate * inverse
        step = jnp.exp(log_step[layer_params])[:, None]
        lam_re = -decay_rate[layer_params]
        lam_im = frequency[layer_params]
        magnitude = jnp.exp(lam_re * step)
        angle = lam_im * step
        abar_re = magnitude * jnp.cos(angle)
        abar_im = magnitude * jnp.sin(angle)
        denom = lam_re * lam_re + lam_im * lam_im
        num_re = abar_re - 1.0
        zoh_re = (num_re * lam_re + abar_im * lam_im) / denom
        zoh_im = (abar_im * lam_re - num_re * lam_im) / denom
        bbar_re = (
            zoh_re[..., None] * in_real[layer_params] - zoh_im[..., None] * in_imag[layer_params]
        )
        bbar_im = (
            zoh_re[..., None] * in_imag[layer_params] + zoh_im[..., None] * in_real[layer_params]
        )
        grouped = drive.reshape(batch, groups, GS)
        push_re = jnp.einsum("bgc,gpc->bgp", grouped, bbar_re, precision=PRECISION_LEVEL)
        push_im = jnp.einsum("bgc,gpc->bgp", grouped, bbar_im, precision=PRECISION_LEVEL)
        old_re = state_real[layer_params]
        old_im = state_imag[layer_params]
        updated_real = abar_re[None] * old_re - abar_im[None] * old_im + push_re
        updated_imag = abar_re[None] * old_im + abar_im[None] * old_re + push_im
        readout_output = jnp.einsum(
            "zju,jiu->zji",
            updated_real,
            readout_real_matrix[layer_params],
            precision=PRECISION_LEVEL,
        ) - jnp.einsum(
            "zju,jiu->zji",
            updated_imag,
            readout_imag_matrix[layer_params],
            precision=PRECISION_LEVEL,
        )
        readout_output = (
            readout_output + skip_gain[layer_params].reshape(groups, GS)[None] * grouped
        )
        gated = (
            jax.nn.gelu(readout_output.reshape(batch, groups * GS)) * jax.nn.sigmoid(gate)
        ).astype(jnp.bfloat16)
        partial_value = jnp.dot(gated, w_output[layer_params], preferred_element_type=jnp.float32)
        outs_re.append(updated_real)
        outs_im.append(updated_imag)
        if layer_params + 1 < LAYERS:
            summed = lax.psum(partial_value, "tp")
            whole = (xf + summed).astype(jnp.bfloat16)
        else:
            own = lax.dynamic_slice_in_dim(whole, offset, width, 1)
            shard = (own.astype(jnp.float32) + spread(partial_value)).astype(jnp.bfloat16)
    return (shard, jnp.stack(outs_re, axis=0), jnp.stack(outs_im, axis=0))


def solution(mesh):
    placed = (
        P("dp", "tp"),
        P(),
        P(None, "dp", "tp"),
        P(None, "dp", "tp"),
        P(None, "tp", None),
        P(None, "tp", None),
        P(None, "tp", None),
        P(None, "tp"),
        P(None, "tp", None, None),
        P(None, "tp", None, None),
        P(None, "tp", None, None),
        P(None, "tp", None, None),
        P(None, "tp"),
        P(None, "dp", "tp", None),
        P(None, "dp", "tp", None),
    )
    return jax.shard_map(
        on_device,
        mesh=mesh,
        in_specs=placed,
        out_specs=(P("dp", "tp"), P(None, "dp", "tp", None), P(None, "dp", "tp", None)),
        check_vma=False,
    )
```

profile of v0, /device:TPU:0, one launch (start us, length us, event | category | flops | bytes accessed | tf_op | source)
XLA Modules:
  0.0 894.9 jit_solution(3569177894118164036)
XLA Ops:
  7.2 10.3 %fusion.143 = (bf16[1,2112,1536]{2,1,0:T(8,128)(2,1)}, bf16[1,2112,1536]{2,1,0:T(8,128)(2,1)}) fusion(bf16[2,2112,1536]{2,1,0:T(8,128)(2,1)} %param.17), kind=kLoop, calls=%fused_computation.162 | loop fusion | bytes 25952256 | tf_op jit(solution)/shard_map/slice | solution.py:51
  17.6 10.7 %fusion.144 = (bf16[1,2112,1536]{2,1,0:T(8,128)(2,1)}, bf16[1,2112,1536]{2,1,0:T(8,128)(2,1)}) fusion(bf16[2,2112,1536]{2,1,0:T(8,128)(2,1)} %param.18), kind=kLoop, calls=%fused_computation.163 | loop fusion | bytes 25952256 | tf_op jit(solution)/shard_map/slice | solution.py:56
  33.2 34.4 %all-gather.4 = bf16[8,1056,48]{1,2,0:T(8,128)(2,1)S(1)} all-gather(bf16[1,1056,48]{1,2,0:T(8,128)(2,1)S(1)} %bitcast.329), channel_id=1, replica_groups=mesh['tp'=8,'dp'=4] {'tp'}, dimensions={0}, use_global_device_ids=true | all-gather | bytes 912384 | tf_op jit(solution)/shard_map/all_gather | solution.py:12
  70.6 3.5 fusion.145
  76.0 3.5 fusion.146
  81.4 2.2 fusion.148
  86.1 2.1 fusion.147
  91.7 87.8 %all-gather.10.cloned.1.call-done = bf16[1,8448,1536]{2,1,0:T(8,128)(2,1)} async-done(((bf16[1,2112,1536]{2,1,0:T(8,128)(2,1)}), bf16[1,8448,1536]{2,1,0:T(8,128)(2,1)}) %all-gather.10.cloned.1.call-update) | async-done | bytes 25952272 | tf_op jit(solution)/shard_map/all_gather | solution.py:51
  179.5 11.5 %fusion.21 = f32[48,1536]{1,0:T(8,128)S(1)} fusion(bf16[1,8448,1536]{2,1,0:T(8,128)(2,1)} %all-gather.10.cloned.1.call-done, f32[8448,48]{0,1:T(8,128)S(1)} %reshape.330, f32[8448]{0:T(1024)S(1)} %get-tuple-element.13, f32[48]{0:T(128)S(1)} %add_rsqrt_fusion.1), kind=kOutput, calls=%fused_computation.33 | convolution fusion | flops 1246593024 | bytes 27903168 | tf_op jit(solution)/shard_map/dot_general | solution.py:49
  191.4 6.7 bitcast_add_fusion.3
  198.2 3.8 fusion.86
  202.0 3.9 bitcast_add_fusion.2
  206.0 3.8 fusion.81
  210.0 130.3 %all-gather.12.cloned.1.call-done = bf16[1,8448,1536]{2,1,0:T(8,128)(2,1)} async-done(((bf16[1,2112,1536]{2,1,0:T(8,128)(2,1)}), bf16[1,8448,1536]{2,1,0:T(8,128)(2,1)}) %all-gather.12.cloned.1.call-update) | async-done | bytes 25952272 | tf_op jit(solution)/shard_map/all_gather | solution.py:56
  340.3 20.3 %fusion.6 = f32[48,8448]{1,0:T(8,128)} fusion(bf16[2,1536,8448]{2,1,0:T(8,128)(2,1)} %param.19, bf16[1,8448,1536]{2,1,0:T(8,128)(2,1)} %all-gather.12.cloned.1.call-done, f32[48,1536]{1,0:T(8,128)S(1)} %copy.90, f32[8448,48]{0,1:T(8,128)S(1)} %reshape.330, f32[8448]{0:T(1024)S(1)} %get-tuple-element.13, f32[48]{0:T(128)S(1)} %add_rsqrt_fusion.1), kind=kOutput, calls=%fused_computation.6 | convolution fusion | flops 2493259776 | bytes 55477440 | tf_op jit(solution)/shard_map/dot_general | solution.py:102
  361.8 2.3 copy.98
  364.9 1.9 copy.113
  366.8 3.0 copy.114
  374.3 76.9 %all-reduce.2.cloned.1.call-done = f32[48,8448]{1,0:T(8,128)} async-done(((f32[48,8448]{1,0:T(8,128)}), f32[48,8448]{1,0:T(8,128)}) %all-reduce.2.cloned.1.call-update) | async-done | bytes 1622032 | tf_op jit(solution)/shard_map/psum | solution.py:106
  452.9 158.2 %all-gather.14.cloned.1.call-done = bf16[1,8448,1536]{2,1,0:T(8,128)(2,1)} async-done(((bf16[1,2112,1536]{2,1,0:T(8,128)(2,1)}), bf16[1,8448,1536]{2,1,0:T(8,128)(2,1)}) %all-gather.14.cloned.1.call-update) | async-done | bytes 25952272 | tf_op jit(solution)/shard_map/all_gather | solution.py:51
  611.1 12.0 %fusion.42 = f32[48,1536]{1,0:T(8,128)S(1)} fusion(bf16[1,8448,1536]{2,1,0:T(8,128)(2,1)} %all-gather.14.cloned.1.call-done, bf16[48,8448]{1,0:T(8,128)(2,1)S(1)} %get-tuple-element.17, f32[8448]{0:T(1024)S(1)} %copy-done.31, f32[48]{0:T(128)S(1)} %add_rsqrt_fusion), kind=kOutput, calls=%fused_computation.40 | convolution fusion | flops 1246998528 | bytes 27092160 | tf_op jit(solution)/shard_map/dot_general | solution.py:49
  623.4 6.6 bitcast_add_fusion.1
  630.0 3.8 fusion.83
  633.8 4.0 bitcast_add_fusion
  637.9 4.0 fusion.79
  642.2 129.5 %all-gather.16.cloned.1.call-done = bf16[1,8448,1536]{2,1,0:T(8,128)(2,1)} async-done(((bf16[1,2112,1536]{2,1,0:T(8,128)(2,1)}), bf16[1,8448,1536]{2,1,0:T(8,128)(2,1)}) %all-gather.16.cloned.1.call-update) | async-done | bytes 25952272 | tf_op jit(solution)/shard_map/all_gather | solution.py:56
  771.7 22.6 %fusion.14 = f32[8448,48]{1,0:T(8,128)} fusion(bf16[2,1536,8448]{2,1,0:T(8,128)(2,1)} %param.19, bf16[1,8448,1536]{2,1,0:T(8,128)(2,1)} %all-gather.16.cloned.1.call-done, bf16[48,8448]{1,0:T(8,128)(2,1)S(1)} %copy-done.12, f32[8448]{0:T(1024)S(1)} %copy-done.31, f32[48,1536]{1,0:T(8,128)S(1)} %copy.104, f32[48]{0:T(128)S(1)} %add_rsqrt_fusion), kind=kOutput, calls=%fused_computation.14 | convolution fusion | flops 2493665280 | bytes 54666432
  796.0 4.1 pad_maximum_fusion.1
  800.1 5.7 copy.106
  805.8 4.1 pad_maximum_fusion
  809.9 5.8 copy.105
  815.7 69.0 %reduce-scatter.4.cloned.1.call-done = f32[1056,48]{1,0:T(8,128)} async-done(((f32[8448,48]{1,0:T(8,128)}), f32[1056,48]{1,0:T(8,128)}) %reduce-scatter.4.cloned.1.call-update) | async-done | bytes 202768
  (127 shorter events, 31.6 us)
Async XLA Ops:
  7.2 172.4 %all-gather.10.cloned.1.call-start = ((), (), s32[]{:S(2)}) async-start(), calls=%async_computation.2 | async-start | bytes 32440320 | tf_op jit(solution)/shard_map/all_gather | solution.py:51
  17.5 322.8 %all-gather.12.cloned.1.call-start = ((), (), s32[]{:S(2)}) async-start(), calls=%async_computation.3 | async-start | bytes 32440320 | tf_op jit(solution)/shard_map/all_gather | solution.py:56
  28.3 422.9 %all-reduce.2.cloned.1.call-start = ((), (), s32[]{:S(2)}) async-start(), calls=%async_computation.1 | async-start | bytes 3244032 | tf_op jit(solution)/shard_map/psum | solution.py:106
  84.8 4.7 copy-start.39
  84.8 6.0 copy-start.37
  179.5 11.8 %copy-start.13 = (f32[96,64,16]{1,2,0:T(8,128)S(1)}, f32[96,64,16]{1,2,0:T(8,128)}, u32[]{:S(2)}) copy-start(f32[96,64,16]{1,2,0:T(8,128)} %copy.82) | copy-start | bytes 1179652
  191.3 6.8 copy-start.19
  191.4 10.6 %copy-start.9 = (f32[1,48,96,64]{3,1,2,0:T(8,128)S(1)}, f32[1,48,96,64]{3,1,2,0:T(8,128)}, u32[]{:S(2)}) copy-start(f32[1,48,96,64]{3,1,2,0:T(8,128)} %copy.110) | copy-start | bytes 3538948
  198.1 7.8 copy-start
  198.1 3.8 copy-start.7
  198.1 3.8 copy-start.15
  198.2 3.8 copy-start.26
  198.2 3.8 copy-start.27
  202.0 4.0 copy-start.17
  202.0 4.0 copy-start.33
  360.6 250.5 %all-gather.14.cloned.1.call-start = ((), (), s32[]{:S(2)}) async-start(), calls=%async_computation.4 | async-start | bytes 32440320 | tf_op jit(solution)/shard_map/all_gather | solution.py:51
  361.2 410.5 %all-gather.16.cloned.1.call-start = ((), (), s32[]{:S(2)}) async-start(), calls=%async_computation.5 | async-start | bytes 32440320 | tf_op jit(solution)/shard_map/all_gather | solution.py:56
  361.7 523.0 %reduce-scatter.4.cloned.1.call-start = ((), (), s32[]{:S(2)}) async-start(), calls=%async_computation.6 | async-start | bytes 4866048
  366.8 4.4 copy-start.22
  366.8 5.6 copy-start.23
  373.6 237.5 %copy-start.31 = (f32[8448]{0:T(1024)S(1)}, f32[8448]{0:T(1024)}, u32[]{:S(2)}) copy-start(f32[8448]{0:T(1024)} %get-tuple-element.12) | copy-start | bytes 101380
  452.9 158.2 %copy-start.11 = (bf16[48,8448]{1,0:T(8,128)(2,1)}, bf16[48,8448]{1,0:T(8,128)(2,1)S(1)}, u32[]{:S(2)}) copy-start(bf16[48,8448]{1,0:T(8,128)(2,1)S(1)} %get-tuple-element.17) | copy-start | bytes 2433028
  611.1 12.2 %copy-start.6 = (f32[1,48,96,64]{3,1,2,0:T(8,128)S(1)}, f32[1,48,96,64]{3,1,2,0:T(8,128)}, u32[]{:S(2)}) copy-start(f32[1,48,96,64]{3,1,2,0:T(8,128)} %copy.113) | copy-start | bytes 3538948
  623.4 6.6 copy-start.18
  630.0 7.9 copy-start.4
  630.0 3.8 copy-start.8
  630.0 3.8 copy-start.14
  633.8 4.0 copy-start.16
  633.8 4.0 copy-start.32
  637.9 4.1 copy-start.5
  637.9 133.8 %copy-start.12 = (bf16[48,8448]{1,0:T(8,128)(2,1)S(1)}, bf16[48,8448]{1,0:T(8,128)(2,1)}, u32[]{:S(2)}) copy-start(bf16[48,8448]{1,0:T(8,128)(2,1)} %copy-done.11) | copy-start | bytes 2433028
  800.1 5.7 copy-start.1
  (15 other events, 38.1 us)
Sparse Core Ops, SparseCore 0:
  17.6 161.8 all-gather.9
  181.1 159.1 all-gather.11
  360.7 90.4 all-reduce.1
  452.6 158.4 all-gather.13
  612.5 159.1 all-gather.15
  794.4 90.2 reduce-scatter.3
where the time goes:
time: 902 us; the launch traced here: 895 us
  waiting for transfers between devices  653 us (72%)
  matrix products  103 us (11%)
  local copies, waits for them, and re-layouts  75.2 us (8%)
  blocking collectives  34.4 us (4%)
  between operations  15 us (2%)
  other arithmetic  14.3 us (2%)
    all_gather x2, waiting for transfers between devices, on_device(): lax.all_gather(w_gating[layer_params], 'dp', axis=0, tiled=True)  260 us
    all_gather x2, waiting for transfers between devices, on_device(): lax.all_gather(w_input[layer_params], 'dp', axis=0, tiled=True)  246 us
    psum x1, waiting for transfers between devices, on_device(): summed = lax.psum(partial_value, 'tp')  76.9 us
    unnamed x7, waiting for transfers between devices  70.1 us
    all_gather x1, blocking collectives, collect(): return lax.all_gather(shard, 'tp', axis=1, tiled=True)  34.4 us
    unnamed x93, local copies, waits for them, and re-layouts  30.1 us
    dot_general x2, matrix products, on_device(): jnp.dot(scaled, lax.all_gather(w_input[layer_params], 'dp', axis=0, tiled...  23.5 us
    unnamed x1, matrix products  22.6 us
  transfers between devices with their start and end apart: 6, of which 6 were waited for; matrix products, arithmetic and copies ran while one was open for 15% of the time, Pallas kernels for 0%

commit v1 on v0

--- a/solution.py
+++ b/solution.py
@@ -2,6 +2,7 @@
 import jax.numpy as jnp
 from jax import lax
 from jax.sharding import PartitionSpec as P
+from jax.lax import all_gather
 
 GS = 16
 LAYERS = 2
@@ -103,7 +104,8 @@
         outs_re.append(updated_real)
         outs_im.append(updated_imag)
         if layer_params + 1 < LAYERS:
-            summed = lax.psum(partial_value, "tp")
+            take_chunk_on = lambda vec: jnp.sum(all_gather(vec, "tp"), axis=0)
+            summed = take_chunk_on(partial_value)
             whole = (xf + summed).astype(jnp.bfloat16)
         else:
             own = lax.dynamic_slice_in_dim(whole, offset, width, 1)

time: 902 us -> 991 us (1.099)
  waiting for transfers between devices: 653 us -> 738 us
    all_gather x0 -> x1, waiting for transfers between devices: none -> 168 us  [on_device(): take_chunk_on = lambda vec: jnp.sum(all_gather(vec, 'tp'), axis=0)]
    psum x1 -> x0, waiting for transfers between devices: 76.9 us -> none  [on_device(): summed = lax.psum(partial_value, 'tp')]
    unnamed x93 -> x87, local copies, waits for them, and re-layouts: 30.1 us -> 30.2 us
  transfers between devices with their start and end apart: 6 -> 6, of which waited for: 6 -> 6; matrix products, arithmetic and copies ran while one was open for 15% -> 14% of each run, Pallas kernels for 0% -> 0%
where the time goes in v1:
time: 991 us; the launch traced here: 984 us
  waiting for transfers between devices  738 us (74%)
  matrix products  104 us (10%)
  local copies, waits for them, and re-layouts  74.1 us (7%)
  blocking collectives  34.4 us (3%)
  other arithmetic  19.2 us (2%)
  between operations  14.8 us (1%)
    all_gather x2, waiting for transfers between devices, on_device(): lax.all_gather(w_gating[layer_params], 'dp', axis=0, tiled=True)  259 us
    all_gather x2, waiting for transfers between devices, on_device(): lax.all_gather(w_input[layer_params], 'dp', axis=0, tiled=True)  240 us
    all_gather x1, waiting for transfers between devices, on_device(): take_chunk_on = lambda vec: jnp.sum(all_gather(vec, 'tp'), axis=0)  168 us
    unnamed x7, waiting for transfers between devices  70.1 us
    all_gather x1, blocking collectives, collect(): return lax.all_gather(shard, 'tp', axis=1, tiled=True)  34.4 us
    unnamed x87, local copies, waits for them, and re-layouts  30.2 us
    dot_general x2, matrix products, on_device(): jnp.dot(scaled, lax.all_gather(w_input[layer_params], 'dp', axis=0, tiled...  24.1 us
    unnamed x1, matrix products  22.6 us
  transfers between devices with their start and end apart: 6, of which 6 were waited for; matrix products, arithmetic and copies ran while one was open for 14% of the time, Pallas kernels for 0%

profile of v1, /device:TPU:0, one launch (start us, length us, event | category | flops | bytes accessed | tf_op | source)
XLA Modules:
  0.0 984.0 jit_solution(9917616298487372663)
XLA Ops:
  7.2 10.3 %fusion.143 = (bf16[1,2112,1536]{2,1,0:T(8,128)(2,1)}, bf16[1,2112,1536]{2,1,0:T(8,128)(2,1)}) fusion(bf16[2,2112,1536]{2,1,0:T(8,128)(2,1)} %param.17), kind=kLoop, calls=%fused_computation.162 | loop fusion | bytes 25952256 | tf_op jit(solution)/shard_map/slice | solution.py:52
  17.6 10.7 %fusion.144 = (bf16[1,2112,1536]{2,1,0:T(8,128)(2,1)}, bf16[1,2112,1536]{2,1,0:T(8,128)(2,1)}) fusion(bf16[2,2112,1536]{2,1,0:T(8,128)(2,1)} %param.18), kind=kLoop, calls=%fused_computation.163 | loop fusion | bytes 25952256 | tf_op jit(solution)/shard_map/slice | solution.py:57
  33.1 34.4 %all-gather.5 = bf16[8,1056,48]{1,2,0:T(8,128)(2,1)S(1)} all-gather(bf16[1,1056,48]{1,2,0:T(8,128)(2,1)S(1)} %bitcast.331), channel_id=1, replica_groups=mesh['tp'=8,'dp'=4] {'tp'}, dimensions={0}, use_global_device_ids=true | all-gather | bytes 912384 | tf_op jit(solution)/shard_map/all_gather | solution.py:13
  70.5 3.4 fusion.145
  75.9 3.5 fusion.146
  81.3 2.2 fusion.148
  86.1 2.1 fusion.147
  91.1 88.4 %all-gather.12.cloned.1.call-done = bf16[1,8448,1536]{2,1,0:T(8,128)(2,1)} async-done(((bf16[1,2112,1536]{2,1,0:T(8,128)(2,1)}), bf16[1,8448,1536]{2,1,0:T(8,128)(2,1)}) %all-gather.12.cloned.1.call-update) | async-done | bytes 25952272 | tf_op jit(solution)/shard_map/all_gather | solution.py:52
  179.5 11.5 %fusion.21 = f32[48,1536]{1,0:T(8,128)S(1)} fusion(bf16[1,8448,1536]{2,1,0:T(8,128)(2,1)} %all-gather.12.cloned.1.call-done, f32[8448,48]{0,1:T(8,128)S(1)} %reshape.331, f32[8448]{0:T(1024)S(1)} %get-tuple-element.16, f32[48]{0:T(128)S(1)} %add_rsqrt_fusion.1), kind=kOutput, calls=%fused_computation.33 | convolution fusion | flops 1246593024 | bytes 27903168 | tf_op jit(solution)/shard_map/dot_general | solution.py:50
  191.4 6.7 bitcast_add_fusion.3
  198.2 3.8 fusion.86
  202.0 3.9 bitcast_add_fusion.2
  206.0 3.8 fusion.81
  210.0 130.3 %all-gather.14.cloned.1.call-done = bf16[1,8448,1536]{2,1,0:T(8,128)(2,1)} async-done(((bf16[1,2112,1536]{2,1,0:T(8,128)(2,1)}), bf16[1,8448,1536]{2,1,0:T(8,128)(2,1)}) %all-gather.14.cloned.1.call-update) | async-done | bytes 25952272 | tf_op jit(solution)/shard_map/all_gather | solution.py:57
  340.3 20.3 %fusion.6 = f32[48,8448]{1,0:T(8,128)} fusion(bf16[2,1536,8448]{2,1,0:T(8,128)(2,1)} %param.19, bf16[1,8448,1536]{2,1,0:T(8,128)(2,1)} %all-gather.14.cloned.1.call-done, f32[48,1536]{1,0:T(8,128)S(1)} %copy.120, f32[8448,48]{0,1:T(8,128)S(1)} %reshape.331, f32[8448]{0:T(1024)S(1)} %get-tuple-element.16, f32[48]{0:T(128)S(1)} %add_rsqrt_fusion.1), kind=kOutput, calls=%fused_computation.6 | convolution fusion | flops 2493259776 | bytes 55477440 | tf_op jit(solution)/shard_map/dot_general | solution.py:103
  361.8 2.3 copy.128
  366.2 3.0 copy.144
  373.8 167.9 %all-gather.16.cloned.1.call-done = f32[384,8448]{1,0:T(8,128)} async-done(((f32[48,8448]{1,0:T(8,128)}), f32[384,8448]{1,0:T(8,128)}) %all-gather.16.cloned.1.call-update) | async-done | bytes 12976144 | tf_op jit(solution)/shard_map/all_gather | solution.py:107
  541.6 5.5 reduce_sum.28
  548.3 152.1 %all-gather.18.cloned.1.call-done = bf16[1,8448,1536]{2,1,0:T(8,128)(2,1)} async-done(((bf16[1,2112,1536]{2,1,0:T(8,128)(2,1)}), bf16[1,8448,1536]{2,1,0:T(8,128)(2,1)}) %all-gather.18.cloned.1.call-update) | async-done | bytes 25952272 | tf_op jit(solution)/shard_map/all_gather | solution.py:52
  700.4 12.6 %fusion.42 = f32[48,1536]{1,0:T(8,128)S(1)} fusion(bf16[1,8448,1536]{2,1,0:T(8,128)(2,1)} %all-gather.18.cloned.1.call-done, bf16[48,8448]{1,0:T(8,128)(2,1)} %get-tuple-element.20, f32[8448]{0:T(1024)} %get-tuple-element.15, f32[48]{0:T(128)S(1)} %add_rsqrt_fusion), kind=kOutput, calls=%fused_computation.40 | convolution fusion | flops 1246998528 | bytes 27092160 | tf_op jit(solution)/shard_map/dot_general | solution.py:50
  713.3 6.8 bitcast_add_fusion.1
  720.1 3.8 fusion.83
  723.9 4.0 bitcast_add_fusion
  727.9 3.9 fusion.79
  732.1 128.9 %all-gather.20.cloned.1.call-done = bf16[1,8448,1536]{2,1,0:T(8,128)(2,1)} async-done(((bf16[1,2112,1536]{2,1,0:T(8,128)(2,1)}), bf16[1,8448,1536]{2,1,0:T(8,128)(2,1)}) %all-gather.20.cloned.1.call-update) | async-done | bytes 25952272 | tf_op jit(solution)/shard_map/all_gather | solution.py:57
  861.0 22.6 %fusion.14 = f32[8448,48]{1,0:T(8,128)} fusion(bf16[2,1536,8448]{2,1,0:T(8,128)(2,1)} %param.19, bf16[1,8448,1536]{2,1,0:T(8,128)(2,1)} %all-gather.20.cloned.1.call-done, bf16[48,8448]{1,0:T(8,128)(2,1)S(1)} %copy-done.11, f32[8448]{0:T(1024)S(1)} %copy-done.29, f32[48,1536]{1,0:T(8,128)S(1)} %copy.134, f32[48]{0:T(128)S(1)} %add_rsqrt_fusion), kind=kOutput, calls=%fused_computation.14 | convolution fusion | flops 2493665280 | bytes 54666432
  885.3 4.1 pad_maximum_fusion.1
  889.4 5.7 copy.136
  895.1 4.1 pad_maximum_fusion
  899.2 5.8 copy.135
  905.0 69.0 %reduce-scatter.4.cloned.1.call-done = f32[1056,48]{1,0:T(8,128)} async-done(((f32[8448,48]{1,0:T(8,128)}), f32[1056,48]{1,0:T(8,128)}) %reduce-scatter.4.cloned.1.call-update) | async-done | bytes 202768
  (122 shorter events, 31.8 us)
Async XLA Ops:
  7.2 172.4 %all-gather.12.cloned.1.call-start = ((), (), s32[]{:S(2)}) async-start(), calls=%async_computation.1 | async-start | bytes 32440320 | tf_op jit(solution)/shard_map/all_gather | solution.py:52
  17.5 322.7 %all-gather.14.cloned.1.call-start = ((), (), s32[]{:S(2)}) async-start(), calls=%async_computation.2 | async-start | bytes 32440320 | tf_op jit(solution)/shard_map/all_gather | solution.py:57
  28.3 513.3 %all-gather.16.cloned.1.call-start = ((), (), s32[]{:S(2)}) async-start(), calls=%async_computation.3 | async-start | bytes 14598144 | tf_op jit(solution)/shard_map/all_gather | solution.py:107
  84.8 4.7 copy-start.36
  84.8 5.4 copy-start.35
  179.5 11.8 %copy-start.12 = (f32[96,64,16]{1,2,0:T(8,128)S(1)}, f32[96,64,16]{1,2,0:T(8,128)}, u32[]{:S(2)}) copy-start(f32[96,64,16]{1,2,0:T(8,128)} %copy.112) | copy-start | bytes 1179652
  191.3 6.8 copy-start.18
  191.3 10.6 %copy-start.9 = (f32[1,48,96,64]{3,1,2,0:T(8,128)S(1)}, f32[1,48,96,64]{3,1,2,0:T(8,128)}, u32[]{:S(2)}) copy-start(f32[1,48,96,64]{3,1,2,0:T(8,128)} %copy.140) | copy-start | bytes 3538948
  198.1 7.8 copy-start
  198.1 3.8 copy-start.8
  198.1 3.8 copy-start.14
  198.2 3.8 copy-start.25
  198.2 3.8 copy-start.26
  202.0 4.0 copy-start.17
  202.0 4.0 copy-start.31
  206.0 3.8 copy-start.2
  360.6 339.8 %all-gather.18.cloned.1.call-start = ((), (), s32[]{:S(2)}) async-start(), calls=%async_computation.4 | async-start | bytes 32440320 | tf_op jit(solution)/shard_map/all_gather | solution.py:52
  361.2 499.8 %all-gather.20.cloned.1.call-start = ((), (), s32[]{:S(2)}) async-start(), calls=%async_computation.5 | async-start | bytes 32440320 | tf_op jit(solution)/shard_map/all_gather | solution.py:57
  361.7 612.3 %reduce-scatter.4.cloned.1.call-start = ((), (), s32[]{:S(2)}) async-start(), calls=%async_computation.6 | async-start | bytes 4866048
  366.2 4.4 copy-start.21
  366.2 5.6 copy-start.22
  700.4 12.8 %copy-start.6 = (f32[1,48,96,64]{3,1,2,0:T(8,128)S(1)}, f32[1,48,96,64]{3,1,2,0:T(8,128)}, u32[]{:S(2)}) copy-start(f32[1,48,96,64]{3,1,2,0:T(8,128)} %copy.143) | copy-start | bytes 3538948
  713.2 6.8 copy-start.16
  720.0 7.8 copy-start.4
  720.0 3.8 copy-start.7
  720.1 3.8 copy-start.13
  723.8 4.0 copy-start.15
  723.8 4.0 copy-start.30
  727.9 4.0 copy-start.5
  727.9 133.1 %copy-start.11 = (bf16[48,8448]{1,0:T(8,128)(2,1)S(1)}, bf16[48,8448]{1,0:T(8,128)(2,1)}, u32[]{:S(2)}) copy-start(bf16[48,8448]{1,0:T(8,128)(2,1)} %get-tuple-element.20) | copy-start | bytes 2433028
  727.9 133.1 %copy-start.29 = (f32[8448]{0:T(1024)S(1)}, f32[8448]{0:T(1024)}, u32[]{:S(2)}) copy-start(f32[8448]{0:T(1024)} %get-tuple-element.15) | copy-start | bytes 101380
  889.4 5.7 copy-start.1
  (12 other events, 26.2 us)
Sparse Core Ops, SparseCore 0:
  17.6 161.8 all-gather.11
  181.1 159.1 all-gather.13
  360.7 180.8 all-gather.15
  543.1 157.2 all-gather.17
  701.8 159.1 all-gather.19
  883.7 90.2 reduce-scatter.3
